TPU v7x, 32 devices: a whole 2x2x4 slice. The times are simulated.
32 devices in a mesh: sp: 4 (over z), fs: 4 (over y, x), tp: 2 (over core).
Axes of the slice: x: 2, y: 2, z: 4, core: 2. Of those that a mesh axis runs over, the one named last changes fastest.
Arguments:
- tokens: bfloat16 [4, 2048, 2048], P('fs', 'sp', 'tp'), may hold values from -6 to 6
- norm_gain: float32 [2048], replicated, may hold values from 0.1 to 1.9
- query_weight: bfloat16 [2048, 1024], P(('sp', 'fs'), 'tp'), may hold values from -0.125 to 0.125
- key_weight: bfloat16 [2048, 1024], P(('sp', 'fs'), 'tp'), may hold values from -0.125 to 0.125
- value_weight: bfloat16 [2048, 2048], P(('sp', 'fs'), 'tp'), may hold values from -0.125 to 0.125
- outgate_weight: bfloat16 [2048, 2048], P(('sp', 'fs'), 'tp'), may hold values from -0.125 to 0.125
- gate_weight: bfloat16 [2048, 2, 16], P(('sp', 'fs'), None, 'tp'), may hold values from -6 to 6
- forget_bias: float32 [16], P('tp')
- forget_shift: float32 [4, 16, 2048], P('fs', 'tp', 'sp'), may hold values from -1.5 to 0
- head_norm_gain: float32 [2048], P('tp'), may hold values from 0.1 to 1.9
- exit_weight: bfloat16 [2048, 2048], P(('sp', 'fs'), 'tp'), may hold values from -0.125 to 0.125
- entry_weight: bfloat16 [2048, 2048], P(('sp', 'fs'), 'tp'), may hold values from -0.125 to 0.125
- signal_weight: bfloat16 [2048, 2048], P(('sp', 'fs'), 'tp'), may hold values from -0.125 to 0.125
- conv_kernel: float32 [3, 2048], P(None, 'tp'), may hold values from -3.5 to 3.5
- merge_weight: bfloat16 [4096, 2048], P(('sp', 'fs'), 'tp'), may hold values from -0.09375 to 0.09375
Outputs:
- mixed: bfloat16 [4, 2048, 2048], P('fs', 'sp', 'tp')
All inputs are finite; a program needn't handle non-finite values.
Results may differ from a plain program's by a relative error of at most 0.017.
The roundings to bfloat16 on the way count: a program that leaves them out, or rounds other values in their place, can miss the bound.
Values may be sent and summed in bfloat16 or wider, within the bound.
A program may use at most 128 MiB of HBM per device.

v0:
```python
import jax
import jax.numpy as jnp
from jax import lax
from jax.sharding import PartitionSpec as P

DK = 64
DV = 128
BLOCK = 128
KERNEL = 3


EPSILON = 1e-06
EMPTY_LOG = -1e30
HIGHEST = lax.Precision.HIGHEST


def prefix(part, axis, combine, identity):
    place = lax.axis_index(axis)
    gathered = jax.tree.map(lambda a: lax.all_gather(a, axis), part)
    state = jax.tree.map(lambda a, e: jnp.zeros_like(a) + jnp.asarray(e, a.dtype), part, identity)

    def one(step, state):
        return combine(
            state, jax.tree.map(lambda a: lax.dynamic_index_in_dim(a, step, 0, False), gathered)
        )

    return lax.fori_loop(0, place, one, state)


def passed_along(value, axis, steps):
    count = lax.axis_size(axis)
    initial, last = (max(0, -steps), min(count, count - steps))
    return lax.ppermute(value, axis, [(source, source + steps) for source in range(initial, last)])


def combine(earlier, later):
    ceiling = jnp.maximum(later[2] + earlier[1], later[1])
    kept = jnp.exp(later[2] + earlier[1] - ceiling)
    added = jnp.exp(later[1] - ceiling)
    state = kept[..., None, None] * earlier[0] + added[..., None, None] * later[0]
    return (state, ceiling, earlier[2] + later[2])


def identity_state(heads):
    return (
        jnp.zeros((heads, DK, DV), jnp.float32),
        jnp.full((heads,), EMPTY_LOG, jnp.float32),
        jnp.zeros((heads,), jnp.float32),
    )


def add_product(left, piece):
    return jnp.dot(left, piece, preferred_element_type=jnp.float32)


def split_columns(total, stack):
    outputs = []
    offset = 0
    for weight in stack:
        outputs.append(total[:, offset : offset + weight.shape[1]])
        offset = offset + weight.shape[1]
    return outputs


def incoming_state(running):
    heads = running[1].shape[0]
    before = prefix((running[0], running[1], running[2]), "sp", combine, identity_state(heads))
    ceiling = jnp.maximum(before[1], before[2])
    shrink = jnp.exp(before[1] - ceiling)
    return (before[0] * shrink[:, None, None], ceiling, before[2])


def memory_states(keys, values, gates, forget_bias, forget_shift):
    count = gates.shape[0]
    heads = forget_bias.shape[0]
    blocks = count // BLOCK
    inputs = gates[:, :heads].reshape(blocks, BLOCK, heads)
    logs = jax.nn.log_sigmoid(gates[:, heads:] + forget_bias) + forget_shift[0].T
    cumulative = jnp.cumsum(logs.reshape(blocks, BLOCK, heads), axis=1)
    last = cumulative[:, -1]
    weight_logs = last[:, None, :] - cumulative + inputs
    peak = jnp.max(weight_logs, axis=1)
    coefficient_array = jnp.exp(weight_logs - peak[:, None, :])
    scaled = keys.reshape(blocks, BLOCK, heads, DK).astype(jnp.float32) * DK ** (-0.5)
    value_float = values.reshape(blocks, BLOCK, heads, DV).astype(jnp.float32)
    states = jnp.einsum(
        "csh,cshk,cshv->chkv", coefficient_array, scaled, value_float, precision=HIGHEST
    )
    running = identity_state(heads)
    prefixes = []
    for index in range(blocks):
        prefixes.append(running)
        running = combine(running, (states[index], peak[index], last[index]))
    leading_part = tuple((jnp.stack([item[member] for item in prefixes]) for member in range(3)))
    gate_apertures = combine(incoming_state(running), leading_part)
    return (gate_apertures, cumulative, inputs)


def memory_output(
    queries, keys, values, outgates, inputs, cumulative, gate_apertures, head_norm_gain
):
    blocks = cumulative.shape[0]
    heads = cumulative.shape[2]
    count = queries.shape[0]
    query_blocks = queries.reshape(blocks, BLOCK, heads, DK)
    key_blocks = keys.reshape(blocks, BLOCK, heads, DK)
    value_blocks = values.reshape(blocks, BLOCK, heads, DV)
    score_matrix = jnp.einsum(
        "cjhk,cshk->chjs", query_blocks, key_blocks, preferred_element_type=jnp.float32
    ) * DK ** (-0.5)
    cum_lanes = cumulative.transpose(0, 2, 1)
    input_lanes = inputs.transpose(0, 2, 1)
    causal = jnp.tril(jnp.ones((BLOCK, BLOCK), dtype=bool))
    decay = jnp.where(
        causal,
        cum_lanes[..., :, None] - cum_lanes[..., None, :] + input_lanes[..., None, :],
        -jnp.inf,
    )
    inter = cum_lanes + gate_apertures[1][..., None]
    ceiling = jnp.maximum(inter, jnp.max(decay, axis=-1))
    weighted = score_matrix * jnp.exp(decay - ceiling[..., None])
    numerator = jnp.einsum(
        "chjs,cshv->chjv",
        weighted.astype(jnp.bfloat16),
        value_blocks,
        preferred_element_type=jnp.float32,
    )
    query_float = query_blocks.astype(jnp.float32)
    carried = jnp.exp(inter - ceiling)
    numerator = numerator + carried[..., None] * jnp.einsum(
        "cjhk,chkv->chjv", query_float, gate_apertures[0], precision=HIGHEST
    )
    result = numerator * lax.rsqrt(
        jnp.mean(numerator * numerator, axis=-1, keepdims=True) + EPSILON
    )
    result = result.transpose(0, 2, 1, 3).reshape(count, heads * DV) * head_norm_gain
    return (result * jax.nn.sigmoid(outgates.astype(jnp.float32))).astype(jnp.bfloat16)


def local(
    tokens,
    norm_gain,
    query_weight,
    key_weight,
    value_weight,
    outgate_weight,
    gate_weight,
    forget_bias,
    forget_shift,
    head_norm_gain,
    exit_weight,
    entry_weight,
    signal_weight,
    conv_kernel,
    merge_weight,
):
    whole = lax.all_gather(tokens, "tp", axis=2, tiled=True)[0]
    count = whole.shape[0]
    flat = whole.astype(jnp.float32)
    normed = (
        flat * lax.rsqrt(jnp.mean(flat * flat, axis=-1, keepdims=True) + EPSILON) * norm_gain
    ).astype(jnp.bfloat16)
    gate_rows = gate_weight.reshape(gate_weight.shape[0], -1)
    state_stack = [key_weight, value_weight, gate_rows]
    other_stack = [query_weight, outgate_weight, exit_weight, entry_weight, signal_weight]
    stacked = jnp.concatenate(state_stack + other_stack, axis=1)
    total = add_product(normed, lax.all_gather(stacked, ("sp", "fs"), axis=0, tiled=True))
    columns = split_columns(total, state_stack + other_stack)
    keys = columns[0].astype(jnp.bfloat16)
    values = columns[1].astype(jnp.bfloat16)
    gate_apertures, cumulative, inputs = memory_states(
        keys, values, columns[2], forget_bias, forget_shift
    )
    others = columns[3:]
    queries = others[0].astype(jnp.bfloat16)
    outgates = others[1].astype(jnp.bfloat16)
    exit_rows = others[2].astype(jnp.bfloat16)
    entry_rows = others[3].astype(jnp.bfloat16)
    signal_rows = others[4].astype(jnp.bfloat16)
    mixed_in = (entry_rows.astype(jnp.float32) * signal_rows.astype(jnp.float32)).astype(
        jnp.bfloat16
    )
    rim = passed_along(mixed_in[count - (KERNEL - 1) :], "sp", 1)
    padded = jnp.concatenate([rim, mixed_in], axis=0).astype(jnp.float32)
    response = conv_kernel[0] * padded[0:count]
    for tap in range(1, KERNEL):
        response = response + conv_kernel[tap] * padded[tap : tap + count]
    conv_out = (exit_rows.astype(jnp.float32) * response).astype(jnp.bfloat16)
    memory_out = memory_output(
        queries, keys, values, outgates, inputs, cumulative, gate_apertures, head_norm_gain
    )
    memory_all, conv_all = (
        lax.all_gather(memory_out, "tp", axis=1, tiled=True),
        lax.all_gather(conv_out, "tp", axis=1, tiled=True),
    )
    concatenated_result = jnp.concatenate([memory_all, conv_all], axis=1)
    mixed = add_product(
        concatenated_result, lax.all_gather(merge_weight, ("sp", "fs"), axis=0, tiled=True)
    )
    return mixed.astype(jnp.bfloat16)[None]


def solution(mesh):
    placed = (
        P("fs", "sp", "tp"),
        P(),
        P(("sp", "fs"), "tp"),
        P(("sp", "fs"), "tp"),
        P(("sp", "fs"), "tp"),
        P(("sp", "fs"), "tp"),
        P(("sp", "fs"), None, "tp"),
        P("tp"),
        P("fs", "tp", "sp"),
        P("tp"),
        P(("sp", "fs"), "tp"),
        P(("sp", "fs"), "tp"),
        P(("sp", "fs"), "tp"),
        P(None, "tp"),
        P(("sp", "fs"), "tp"),
    )
    return jax.shard_map(
        local, mesh=mesh, in_specs=placed, out_specs=P("fs", "sp", "tp"), check_vma=False
    )
```

profile of v0, /device:TPU:9, one launch (start us, length us, event | category | flops | bytes accessed | tf_op | source)
XLA Modules:
  0.0 513.4 jit_solution(8808252792740603250)
XLA Ops:
  6.5 0.7 all-gather.9.cloned.1.call-update
  7.3 0.8 copy.62
  8.1 4.0 concatenate.34
  12.2 9.2 %all-gather.9.cloned.1.call-done = bf16[1,512,2048]{2,1,0:T(8,128)(2,1)} async-done(((bf16[1,512,1024]{2,1,0:T(8,128)(2,1)}), bf16[1,512,2048]{2,1,0:T(8,128)(2,1)}) %all-gather.9.cloned.1.call-update) | async-done | bytes 2097168 | tf_op jit(solution)/shard_map/all_gather | solution.py:157
  21.4 2.2 fusion.6
  23.6 273.9 %all-gather.11.cloned.1.call-done = bf16[2048,6160]{1,0:T(8,128)(2,1)} async-done(((bf16[128,6160]{1,0:T(8,128)(2,1)}), bf16[2048,6160]{1,0:T(8,128)(2,1)}) %all-gather.11.cloned.1.call-update) | async-done | bytes 25231376 | tf_op jit(solution)/shard_map/all_gather | solution.py:167
  297.5 21.4 %fusion.102 = (bf16[512,6160]{0,1:T(8,128)(2,1)}, f32[512,6160]{0,1:T(8,128)}) fusion(bf16[2048,6160]{1,0:T(8,128)(2,1)} %all-gather.11.cloned.1.call-done, bf16[1,512,2048]{2,1,0:T(8,128)(2,1)S(1)} %copy-done.1, f32[2048]{0:T(1024)S(1)} %copy-done.6, f32[512]{0:T(512)S(1)} %add_rsqrt_fusion), kind=kOutput, calls=%fused_computation.150 | convolution fusion | flops 12925804544 | bytes 46262272 | tf_op jit(solution)/shard_map/dot_general | solution.py:53
  319.0 0.8 slice_bitcast_fusion
  319.8 0.1 copy.65
  319.9 0.3 reduce_window_sum.11
  320.2 0.1 copy.67
  320.3 0.1 fusion.71
  320.4 0.1 exponential_multiply_fusion
  320.5 1.3 fusion.100
  321.7 1.3 slice.143
  323.0 0.1 copy.69
  323.1 0.1 reshape.510
  323.3 0.3 reshape.513
  323.6 2.2 fusion.44
  325.8 1.1 fusion.67
  327.0 0.5 all-gather.19.cloned.1.call-update
  327.6 7.9 %all-gather = f32[4,1,8]{2,1,0:T(1,128)S(1)} all-gather(f32[1,1,8]{2,1,0:T(1,128)S(1)} %get-tuple-element.101), channel_id=1, replica_groups=mesh['sp'=4,'fs'=4,'tp'=2] {'sp'}, dimensions={0}, use_global_device_ids=true | all-gather | bytes 160 | tf_op jit(solution)/shard_map/all_gather | solution.py:19
  335.6 8.5 %all-gather.1 = f32[4,1,8]{2,1,0:T(1,128)S(1)} all-gather(f32[1,1,8]{2,1,0:T(1,128)S(1)} %get-tuple-element.83), channel_id=1, replica_groups=mesh['sp'=4,'fs'=4,'tp'=2] {'sp'}, dimensions={0}, use_global_device_ids=true | all-gather | bytes 160 | tf_op jit(solution)/shard_map/all_gather | solution.py:19
  344.0 0.1 copy.66
  344.1 1.3 fusion.24
  345.4 0.1 copy.72
  345.6 0.9 reshape.509
  346.5 8.5 %all-gather.13.cloned.1.call-done = f32[4,8,64,128]{3,2,1,0:T(8,128)} async-done(((f32[1,8,64,128]{3,2,1,0:T(8,128)}), f32[4,8,64,128]{3,2,1,0:T(8,128)}) %all-gather.13.cloned.1.call-update) | async-done | bytes 1048592 | tf_op jit(solution)/shard_map/all_gather | solution.py:19
  355.1 1.3 while.14
  355.2 1.1 fusion.110
  356.4 0.1 subtract_exponential_fusion.4
  356.6 0.1 copy.73
  356.7 0.1 subtract_exponential_fusion.2
  356.8 0.1 broadcast_multiply_fusion
  356.9 3.2 fusion.35
  360.1 4.4 multiply_reduce_fusion
  364.5 2.1 fusion.22
  366.6 1.4 copy.75
  367.9 3.5 fusion.16
  371.5 0.1 slice.152
  371.7 4.1 collective-permute-start
  375.8 9.3 %collective-permute-done = bf16[2,1024]{0,1:T(8,128)(2,1)S(1)} collective-permute-done((bf16[2,1024]{0,1:T(8,128)(2,1)S(1)}, bf16[2,1024]{0,1:T(8,128)(2,1)S(1)}, u32[]{:S(2)}, u32[]{:S(2)}) %collective-permute-start) | collective-permute-done | bytes 4128 | tf_op jit(solution)/shard_map/ppermute | solution.py:33
  385.1 0.6 maximum_convert_fusion
  385.7 3.8 fusion.19
  389.5 80.0 %all-gather.19.cloned.1.call-done = bf16[4096,1024]{1,0:T(8,128)(2,1)} async-done(((bf16[256,1024]{1,0:T(8,128)(2,1)}), bf16[4096,1024]{1,0:T(8,128)(2,1)}) %all-gather.19.cloned.1.call-update) | async-done | bytes 8388624 | tf_op jit(solution)/shard_map/all_gather | solution.py:198
  469.6 13.7 %all-gather.15.cloned.1.call-done = bf16[512,2048]{0,1:T(8,128)(2,1)} async-done(((bf16[512,1024]{0,1:T(8,128)(2,1)}), bf16[512,2048]{0,1:T(8,128)(2,1)}) %all-gather.15.cloned.1.call-update) | async-done | bytes 2097168 | tf_op jit(solution)/shard_map/all_gather | solution.py:193
  483.3 13.2 %all-gather.17.cloned.1.call-done = bf16[512,2048]{0,1:T(8,128)(2,1)} async-done(((bf16[512,1024]{0,1:T(8,128)(2,1)}), bf16[512,2048]{0,1:T(8,128)(2,1)}) %all-gather.17.cloned.1.call-update) | async-done | bytes 2097168 | tf_op jit(solution)/shard_map/all_gather | solution.py:194
  496.5 10.1 %fusion.31 = bf16[1,512,1024]{2,1,0:T(8,128)(2,1)} fusion(bf16[4096,1024]{1,0:T(8,128)(2,1)} %all-gather.19.cloned.1.call-done, bf16[512,2048]{0,1:T(8,128)(2,1)} %all-gather.17.cloned.1.call-done, bf16[512,2048]{0,1:T(8,128)(2,1)} %all-gather.15.cloned.1.call-done), kind=kOutput, calls=%fused_computation.44 | convolution fusion | flops 4303880192 | bytes 13631488 | tf_op jit(solution)/shard_map/dot_general | solution.py:53
  (43 shorter events, 0.6 us)
Async XLA Ops:
  6.5 14.8 %all-gather.9.cloned.1.call-start = ((), (), s32[]{:S(2)}) async-start(), calls=%async_computation | async-start | bytes 3145728 | tf_op jit(solution)/shard_map/all_gather | solution.py:157
  7.3 290.3 %all-gather.11.cloned.1.call-start = ((), (), s32[]{:S(2)}) async-start(), calls=%async_computation.1 | async-start | bytes 27295744 | tf_op jit(solution)/shard_map/all_gather | solution.py:167
  12.1 285.4 %copy-start.6 = (f32[2048]{0:T(1024)S(1)}, f32[2048]{0:T(1024)}, u32[]{:S(2)}) copy-start(f32[2048]{0:T(1024)} %param.18) | copy-start | bytes 24580
  12.1 342.9 %all-gather.13.cloned.1.call-start = ((), (), s32[]{:S(2)}) async-start(), calls=%async_computation.2 | async-start | bytes 1310720 | tf_op jit(solution)/shard_map/all_gather | solution.py:19
  21.4 276.2 %copy-start.1 = (bf16[1,512,2048]{2,1,0:T(8,128)(2,1)S(1)}, bf16[1,512,2048]{2,1,0:T(8,128)(2,1)}, u32[]{:S(2)}) copy-start(bf16[1,512,2048]{2,1,0:T(8,128)(2,1)} %all-gather.9.cloned.1.call-done) | copy-start | bytes 6291460
  23.6 295.4 %copy-start.2 = (f32[1,8,512]{2,1,0:T(8,128)S(1)}, f32[1,8,512]{2,1,0:T(8,128)}, u32[]{:S(2)}) copy-start(f32[1,8,512]{2,1,0:T(8,128)} %param.25) | copy-start | bytes 49156
  23.6 295.4 %copy-start.5 = (f32[8]{0:T(128)S(1)}, f32[8]{0:T(128)}, u32[]{:S(2)}) copy-start(f32[8]{0:T(128)} %param.24) | copy-start | bytes 100
  323.3 2.5 copy-start
  327.0 142.6 %all-gather.19.cloned.1.call-start = ((), (), s32[]{:S(2)}) async-start(), calls=%async_computation.5 | async-start | bytes 8912896 | tf_op jit(solution)/shard_map/all_gather | solution.py:198
  327.5 155.8 %all-gather.15.cloned.1.call-start = ((), (), s32[]{:S(2)}) async-start(), calls=%async_computation.3 | async-start | bytes 3145728 | tf_op jit(solution)/shard_map/all_gather | solution.py:193
  366.6 1.4 copy-start.4
  367.9 7.8 %copy-start.3 = (f32[3,1024]{1,0:T(4,128)S(1)}, f32[3,1024]{1,0:T(4,128)}, u32[]{:S(2)}) copy-start(f32[3,1024]{1,0:T(4,128)} %param.30) | copy-start | bytes 36868
  371.5 125.0 %all-gather.17.cloned.1.call-start = ((), (), s32[]{:S(2)}) async-start(), calls=%async_computation.4 | async-start | bytes 3145728 | tf_op jit(solution)/shard_map/all_gather | solution.py:194
  371.7 13.4 %collective-permute-start = (bf16[2,1024]{0,1:T(8,128)(2,1)S(1)}, bf16[2,1024]{0,1:T(8,128)(2,1)S(1)}, u32[]{:S(2)}, u32[]{:S(2)}) collective-permute-start(bf16[2,1024]{0,1:T(8,128)(2,1)S(1)} %slice.152), channel_id=1, source_target_pairs={{0,8},{8,16},{16,24},{1,9},{9,17},{17,25},{2,10},{10,18},{18,26},{... | collective-permute-start | bytes 12296 | tf_op jit(solution)/shard_map/ppermute | solution.py:33
Sparse Core Ops, SparseCore 0:
  8.9 12.4 all-gather.8
  24.1 273.3 all-gather.10
  327.1 27.9 all-gather.12
  357.7 111.8 all-gather.18
  470.9 12.2 all-gather.14
  484.7 11.7 all-gather.16
where the time goes:
time: 515 us; the launch traced here: 513 us
  waiting for transfers between devices  409 us (79%)
  matrix products  41.3 us (8%)
  other arithmetic  17.4 us (3%)
  blocking collectives  16.4 us (3%)
  between operations  13.8 us (3%)
  local copies, waits for them, and re-layouts  10.9 us (2%)
    all_gather x1, waiting for transfers between devices, local(): lax.all_gather(stacked, ('sp', 'fs'), axis=0, tiled=True)  274 us
    all_gather x1, waiting for transfers between devices, local(): lax.all_gather(merge_weight, ('sp', 'fs'), axis=0, tiled=True)  80 us
    dot_general x2, matrix products, add_product(): return jnp.dot(left, piece, preferred_element_type=jnp.float32)  31.6 us
    all_gather x2, blocking collectives, prefix(): gathered = jax.tree.map(lambda a: lax.all_gather(a, axis), part)  16.4 us
    all_gather x1, waiting for transfers between devices, local(): lax.all_gather(memory_out, 'tp', axis=1, tiled=True)  13.7 us
    all_gather x1, waiting for transfers between devices, local(): lax.all_gather(conv_out, 'tp', axis=1, tiled=True)  13.2 us
  transfers between devices with their start and end apart: 7, of which 7 were waited for; matrix products, arithmetic and copies ran while one was open for 6% of the time, Pallas kernels for 0%

commit v1 on v0

--- a/solution.py
+++ b/solution.py
@@ -200,6 +200,129 @@
     return mixed.astype(jnp.bfloat16)[None]
 
 
+def whole_states(keys, values, inputs, logs, blocks):
+    heads = inputs.shape[1]
+    inputs = inputs.reshape(blocks, BLOCK, heads)
+    upto = jnp.tril(jnp.ones((BLOCK, BLOCK), jnp.float32))
+    cumulative = jnp.einsum(
+        "js,csh->cjh", upto, logs.reshape(blocks, BLOCK, heads), precision=HIGHEST
+    )
+    last = cumulative[:, -1]
+    weight_logs = last[:, None, :] - cumulative + inputs
+    peak = jnp.max(weight_logs, axis=1)
+    coefficients = jnp.exp(weight_logs - peak[:, None, :])
+    scaled = keys.reshape(blocks, BLOCK, heads, DK).astype(jnp.float32) * DK ** (-0.5)
+    weighted_keys = scaled * coefficients[..., None]
+    value_float = values.reshape(blocks, BLOCK, heads, DV).astype(jnp.float32)
+    states = jnp.einsum("cshk,cshv->chkv", weighted_keys, value_float, precision=HIGHEST)
+    place = jnp.arange(blocks)
+    between = (place[None, :, None] < place[None, None, :]) & (
+        place[None, None, :] < place[:, None, None]
+    )
+    decay = jnp.sum(jnp.where(between[..., None], last[None, None], 0.0), axis=2) + peak[None]
+    earlier = (place[None, :] < place[:, None])[..., None]
+    decay = jnp.where(earlier, decay, -jnp.inf)
+    start = jnp.sum(jnp.where(earlier, last[None], 0.0), axis=1)
+    ceiling = jnp.maximum(start, jnp.max(decay, axis=1))
+    shares = jnp.exp(decay - ceiling[:, None])
+    before = jnp.einsum("cdh,dhkv->chkv", shares, states, precision=HIGHEST)
+    return ((before, ceiling), cumulative, inputs)
+
+
+def resharded(
+    tokens,
+    norm_gain,
+    query_weight,
+    key_weight,
+    value_weight,
+    outgate_weight,
+    gate_weight,
+    forget_bias,
+    forget_shift,
+    head_norm_gain,
+    exit_weight,
+    entry_weight,
+    signal_weight,
+    conv_kernel,
+    merge_weight,
+):
+    parts = lax.axis_size("sp")
+    place = lax.axis_index("sp")
+    depth = key_weight.shape[0]
+    gates = gate_weight.shape[2]
+    heads = gates // parts
+    stack = [
+        query_weight,
+        key_weight,
+        value_weight,
+        outgate_weight,
+        exit_weight,
+        entry_weight,
+        signal_weight,
+        gate_weight.reshape(depth, 2, parts, heads).transpose(0, 2, 1, 3),
+    ]
+    stacked = jnp.concatenate([w.reshape(depth, parts, -1) for w in stack], axis=2)
+    widths = [w.size // depth // parts for w in stack]
+    sent = lax.all_to_all(stacked.transpose(1, 0, 2), "sp", 0, 0)
+    rows = lax.all_gather(sent, "fs", axis=1)
+    rows = rows.reshape(-1, rows.shape[-1])
+    line = lax.all_gather(tokens[0], "sp", axis=0, tiled=True)
+    whole = lax.all_gather(line, "tp", axis=1, tiled=True)
+    count = whole.shape[0]
+    flat = whole.astype(jnp.float32)
+    normed = (
+        flat * lax.rsqrt(jnp.mean(flat * flat, axis=-1, keepdims=True) + EPSILON) * norm_gain
+    ).astype(jnp.bfloat16)
+    total = add_product(normed, rows)
+    columns = []
+    offset = 0
+    for width in widths:
+        columns.append(total[:, offset : offset + width])
+        offset = offset + width
+    queries, keys, values, outgates, exit_rows, entry_rows, signal_rows = [
+        c.astype(jnp.bfloat16) for c in columns[:7]
+    ]
+    gate_pre = columns[7]
+
+    def own(array, axis, width):
+        return lax.dynamic_slice_in_dim(array, place * width, width, axis)
+
+    shift = lax.all_to_all(forget_shift[0].reshape(parts, heads, -1), "sp", 0, 0)
+    shift = shift.transpose(1, 0, 2).reshape(heads, count)
+    logs = jax.nn.log_sigmoid(gate_pre[:, heads:] + own(forget_bias, 0, heads)) + shift.T
+    blocks = count // BLOCK
+    apertures, cumulative, inputs = whole_states(keys, values, gate_pre[:, :heads], logs, blocks)
+    channels = exit_rows.shape[1]
+    taps = own(conv_kernel, 1, channels)
+    mixed_in = (entry_rows.astype(jnp.float32) * signal_rows.astype(jnp.float32)).astype(
+        jnp.bfloat16
+    )
+    padded = jnp.pad(mixed_in, ((KERNEL - 1, 0), (0, 0))).astype(jnp.float32)
+    response = taps[0] * padded[0:count]
+    for tap in range(1, KERNEL):
+        response = response + taps[tap] * padded[tap : tap + count]
+    conv_out = (exit_rows.astype(jnp.float32) * response).astype(jnp.bfloat16)
+    memory_out = memory_output(
+        queries,
+        keys,
+        values,
+        outgates,
+        inputs,
+        cumulative,
+        apertures,
+        own(head_norm_gain, 0, heads * DV),
+    )
+    both = jnp.concatenate([memory_out, conv_out], axis=1)
+    back = lax.all_to_all(both.reshape(parts, count // parts, -1), "sp", 0, 0)
+    halves = lax.all_gather(back, "tp")
+    memory_width = heads * DV
+    memory_all = halves[..., :memory_width].transpose(2, 0, 1, 3).reshape(count // parts, -1)
+    conv_all = halves[..., memory_width:].transpose(2, 0, 1, 3).reshape(count // parts, -1)
+    merge = lax.all_gather(merge_weight, ("sp", "fs"), axis=0, tiled=True)
+    mixed = add_product(jnp.concatenate([memory_all, conv_all], axis=1), merge)
+    return mixed.astype(jnp.bfloat16)[None]
+
+
 def solution(mesh):
     placed = (
         P("fs", "sp", "tp"),
@@ -218,6 +341,14 @@
         P(None, "tp"),
         P(("sp", "fs"), "tp"),
     )
-    return jax.shard_map(
-        local, mesh=mesh, in_specs=placed, out_specs=P("fs", "sp", "tp"), check_vma=False
-    )
+    sp, tp = mesh.shape["sp"], mesh.shape["tp"]
+
+    def step(*args):
+        heads, channels = args[6].shape[2], args[10].shape[1]
+        even = heads % (sp * tp) == 0 and channels % (sp * tp * 128) == 0
+        body = resharded if even else local
+        return jax.shard_map(
+            body, mesh=mesh, in_specs=placed, out_specs=P("fs", "sp", "tp"), check_vma=False
+        )(*args)
+
+    return step

time: 515 us -> 472 us (0.917)
  waiting for transfers between devices: 409 us -> 210 us
  blocking collectives: 16.4 us -> 129 us
  local copies, waits for them, and re-layouts: 10.9 us -> 52.9 us
    all_gather x6 -> x5, waiting for transfers between devices: 399 us -> 209 us  [the longest x1 102 us: resharded(): merge = lax.all_gather(merge_weight, ('sp', 'fs'), axis=0, tiled=True)]
    all_to_all x0 -> x2, blocking collectives: none -> 129 us  [the longest x1 79 us: resharded(): sent = lax.all_to_all(stacked.transpose(1, 0, 2), 'sp', 0, 0)]
    all_gather x0 -> x2, local copies, waits for them, and re-layouts: none -> 24.1 us  [the longest x1 17.7 us: resharded(): rows = lax.all_gather(sent, 'fs', axis=1)]
    unnamed x14 -> x46, local copies, waits for them, and re-layouts: 0.04 us -> 17.2 us
    all_gather x2 -> x0, blocking collectives: 16.4 us -> none  [prefix(): gathered = jax.tree.map(lambda a: lax.all_gather(a, axis), part)]
    ppermute x1 -> x0, waiting for transfers between devices: 9.31 us -> none  [passed_along(): lax.ppermute(value, axis, [(source, source + steps) for source in range(i...]
    all_to_all x0 -> x1, starting transfers between devices: none -> 6.34 us  [resharded(): lax.all_to_all(forget_shift[0].reshape(parts, heads, -1), 'sp', 0, 0)]
  transfers between devices with their start and end apart: 7 -> 6, of which waited for: 7 -> 4; matrix products, arithmetic and copies ran while one was open for 6% -> 14% of each run, Pallas kernels for 0% -> 0%
where the time goes in v1:
time: 472 us; the launch traced here: 467 us
  waiting for transfers between devices  210 us (44%)
  blocking collectives  129 us (27%)
  local copies, waits for them, and re-layouts  52.9 us (11%)
  matrix products  37.7 us (8%)
  other arithmetic  16.9 us (4%)
  between operations  13.6 us (3%)
  starting transfers between devices  6.5 us (1%)
    all_gather x1, waiting for transfers between devices, resharded(): merge = lax.all_gather(merge_weight, ('sp', 'fs'), axis=0, tiled=True)  102 us
    all_to_all x1, blocking collectives, resharded(): sent = lax.all_to_all(stacked.transpose(1, 0, 2), 'sp', 0, 0)  79 us
    all_gather x1, waiting for transfers between devices, resharded(): rows = lax.all_gather(sent, 'fs', axis=1)  64.3 us
    all_to_all x1, blocking collectives, resharded(): back = lax.all_to_all(both.reshape(parts, count // parts, -1), 'sp', 0, 0)  49.7 us
    dot_general x2, matrix products, add_product(): return jnp.dot(left, piece, preferred_element_type=jnp.float32)  28.4 us
    all_gather x1, waiting for transfers between devices, resharded(): line = lax.all_gather(tokens[0], 'sp', axis=0, tiled=True)  27.7 us
    all_gather x1, local copies, waits for them, and re-layouts, resharded(): rows = lax.all_gather(sent, 'fs', axis=1)  17.7 us
    unnamed x46, local copies, waits for them, and re-layouts  17.2 us
  transfers between devices with their start and end apart: 6, of which 4 were waited for; matrix products, arithmetic and copies ran while one was open for 14% of the time, Pallas kernels for 0%

profile of v1, /device:TPU:9, one launch (start us, length us, event | category | flops | bytes accessed | tf_op | source)
XLA Modules:
  0.0 466.6 jit_solution(17754036155125778785)
XLA Ops:
  6.6 0.7 all-gather.12.cloned.1.call-update
  7.3 1.0 copy.151
  8.3 1.0 copy.152
  9.4 1.1 copy.153
  10.5 0.2 copy.154
  10.7 0.2 copy.155
  10.9 0.2 copy.156
  11.6 79.0 %all_to_all.15 = bf16[4,128,1540]{1,2,0:T(8,128)(2,1)} all-to-all(bf16[4,128,1540]{1,2,0:T(8,128)(2,1)S(1)} %bitcast.143), channel_id=1, replica_groups=mesh['sp'=4,'fs'=4,'tp'=2] {'sp'}, dimensions={0} | all-to-all | bytes 3153920 | tf_op jit(solution)/shard_map/all_to_all | solution.py:266
  90.6 27.7 %all-gather.12.cloned.1.call-done = bf16[1,2048,1024]{2,1,0:T(8,128)(2,1)} async-done(((bf16[1,512,1024]{2,1,0:T(8,128)(2,1)}), bf16[1,2048,1024]{2,1,0:T(8,128)(2,1)}) %all-gather.12.cloned.1.call-update) | async-done | bytes 4194320 | tf_op jit(solution)/shard_map/all_gather | solution.py:269
  118.4 0.7 copy-done.7
  119.1 0.6 reshape_squeeze.3
  119.7 6.3 %all-to-all-start.1 = ((f32[4,2,512]{2,1,0:T(2,128)}), f32[4,2,512]{2,1,0:T(2,128)S(1)}, u32[]{:S(2)}, u32[]{:S(2)}) async-start(f32[4,2,512]{2,1,0:T(2,128)} %reshape_squeeze.3), calls=%async_computation.1 | async-start | bytes 32768 | tf_op jit(solution)/shard_map/all_to_all | solution.py:290
  126.1 0.8 dynamic_slice.10
  126.9 0.9 constant_dynamic-slice_fusion
  127.8 64.3 %all-gather.16.cloned.1.call-done = bf16[4,512,1540]{1,2,0:T(8,128)(2,1)} async-done(((bf16[4,128,1540]{1,2,0:T(8,128)(2,1)}), bf16[4,512,1540]{1,2,0:T(8,128)(2,1)}) %all-gather.16.cloned.1.call-update) | async-done | bytes 6307856 | tf_op jit(solution)/shard_map/all_gather | solution.py:267
  192.1 17.7 %copy.243 = bf16[4,512,1540]{1,0,2:T(4,128)(2,1)S(1)} copy(bf16[4,512,1540]{1,2,0:T(8,128)(2,1)} %all-gather.16.cloned.1.call-done) | data formatting | bytes 12615680 | tf_op jit(solution)/shard_map/all_gather | solution.py:267
  209.8 2.6 pad.9
  212.4 5.3 %copy.191 = bf16[193,8,4,512]{3,1,2,0:T(8,128)(2,1)} copy(bf16[193,8,4,512]{3,2,1,0:T(4,128)(2,1)S(1)} %bitcast.129) | data formatting | bytes 12648448
  217.8 5.2 %fusion = f32[2048]{0:T(1024)S(1)} fusion(bf16[1,2048,2048]{2,1,0:T(8,128)(2,1)} %all-gather.14.cloned.1.call-done), kind=kLoop, calls=%fused_computation.2 | loop fusion | flops 12580864 | bytes 8396800 | tf_op jit(solution)/shard_map/reduce_sum | solution.py:274
  223.0 0.5 copy-done
  223.6 18.9 %fusion.78 = (bf16[2048,1540]{0,1:T(8,128)(2,1)}, f32[2048,1540]{0,1:T(8,128)}) fusion(bf16[2048,1540]{0,1:T(8,128)(2,1)} %bitcast.135, bf16[1,2048,2048]{2,1,0:T(8,128)(2,1)S(1)} %copy-done, f32[2048]{0:T(1024)S(1)} %copy-done.9, f32[2048]{0:T(1024)S(1)} %add_rsqrt_fusion), kind=kOutput, calls=%fused_computation.117 | convolution fusion | flops 12938387456 | bytes 33636352 | tf_op jit(solution)/shard_map/dot_general | solution.py:53
  242.4 1.0 fusion.56
  243.5 0.2 fusion.48
  244.0 0.2 select_reduce_fusion
  244.6 1.3 fusion.20
  246.1 1.3 slice_bitcast_fusion.2
  247.4 1.3 slice_bitcast_fusion
  248.8 0.2 copy.196
  249.1 0.9 copy.177
  250.0 1.0 fusion.31
  251.0 1.6 convolution_bitcast_fusion
  252.7 0.8 copy-done.2
  253.5 1.9 fusion.28
  255.5 4.6 multiply_reduce_fusion
  260.1 2.1 fusion.19
  262.2 1.2 copy.183
  263.5 3.3 fusion.13
  266.7 0.4 pad_convert_fusion
  267.1 2.7 fusion.16
  270.0 0.4 copy.244
  270.4 49.7 %all_to_all.16 = bf16[4,512,512]{1,2,0:T(8,128)(2,1)S(1)} all-to-all(bf16[4,512,512]{1,2,0:T(8,128)(2,1)S(1)} %bitcast.133), channel_id=1, replica_groups=mesh['sp'=4,'fs'=4,'tp'=2] {'sp'}, dimensions={0} | all-to-all | bytes 4194304 | tf_op jit(solution)/shard_map/all_to_all | solution.py:316
  320.1 2.4 copy.185
  322.5 0.5 all-gather.10.cloned.1.call-update
  323.1 15.0 %all-gather.18.cloned.1.call-done = bf16[8,512,512]{2,1,0:T(8,128)(2,1)} async-done(((bf16[4,512,512]{2,1,0:T(8,128)(2,1)}), bf16[8,512,512]{2,1,0:T(8,128)(2,1)}) %all-gather.18.cloned.1.call-update) | async-done | bytes 4194320 | tf_op jit(solution)/shard_map/all_gather | solution.py:317
  338.0 6.4 %copy.186 = bf16[8,512,512]{1,2,0:T(8,128)(2,1)} copy(bf16[8,512,512]{2,1,0:T(8,128)(2,1)} %all-gather.18.cloned.1.call-done) | data formatting | bytes 8388608 | tf_op jit(solution)/shard_map/all_gather | solution.py:317
  344.5 4.0 fusion.77
  348.5 102.1 %all-gather.10.cloned.1.call-done = bf16[4096,1024]{1,0:T(8,128)(2,1)} async-done(((bf16[256,1024]{1,0:T(8,128)(2,1)}), bf16[4096,1024]{1,0:T(8,128)(2,1)}) %all-gather.10.cloned.1.call-update) | async-done | bytes 8388624 | tf_op jit(solution)/shard_map/all_gather | solution.py:321
  450.6 9.5 %fusion.25 = bf16[1,512,1024]{2,1,0:T(8,128)(2,1)} fusion(bf16[4096,1024]{1,0:T(8,128)(2,1)} %all-gather.10.cloned.1.call-done, bf16[512,2048]{0,1:T(8,128)(2,1)} %bitcast.142, bf16[512,2048]{0,1:T(8,128)(2,1)S(1)} %bitcast.141), kind=kOutput, calls=%fused_computation.36 | convolution fusion | flops 4303880192 | bytes 13631488 | tf_op jit(solution)/shard_map/dot_general | solution.py:53
  (64 shorter events, 2.1 us)
Async XLA Ops:
  6.5 4.0 copy-start.3
  6.5 4.2 copy-start.4
  6.5 4.3 copy-start.5
  6.5 4.5 copy-start.6
  6.5 111.8 %all-gather.12.cloned.1.call-start = ((), (), s32[]{:S(2)}) async-start(), calls=%async_computation.4 | async-start | bytes 5242880 | tf_op jit(solution)/shard_map/all_gather | solution.py:269
  6.6 4.7 copy-start.8
  7.3 184.8 %all-gather.16.cloned.1.call-start = ((), (), s32[]{:S(2)}) async-start(), calls=%async_computation.6 | async-start | bytes 7905280 | tf_op jit(solution)/shard_map/all_gather | solution.py:267
  90.6 127.2 %all-gather.14.cloned.1.call-start = ((), (), s32[]{:S(2)}) async-start(), calls=%async_computation.5 | async-start | bytes 12582912 | tf_op jit(solution)/shard_map/all_gather | solution.py:270
  118.3 0.7 copy-start.7
  118.3 7.7 %copy-start.10 = (f32[8]{0:T(128)S(1)}, f32[8]{0:T(128)}, u32[]{:S(2)}) copy-start(f32[8]{0:T(128)} %param.22) | copy-start | bytes 100
  119.7 122.7 %all-to-all-start.1 = ((f32[4,2,512]{2,1,0:T(2,128)}), f32[4,2,512]{2,1,0:T(2,128)S(1)}, u32[]{:S(2)}, u32[]{:S(2)}) async-start(f32[4,2,512]{2,1,0:T(2,128)} %reshape_squeeze.3), calls=%async_computation.1 | async-start | bytes 32768 | tf_op jit(solution)/shard_map/all_to_all | solution.py:290
  126.0 212.0 %all-gather.18.cloned.1.call-start = ((), (), s32[]{:S(2)}) async-start(), calls=%async_computation.7 | async-start | bytes 6291456 | tf_op jit(solution)/shard_map/all_gather | solution.py:317
  217.8 5.3 %copy-start.9 = (f32[2048]{0:T(1024)S(1)}, f32[2048]{0:T(1024)}, u32[]{:S(2)}) copy-start(f32[2048]{0:T(1024)} %param.16) | copy-start | bytes 24580
  217.8 5.8 %copy-start = (bf16[1,2048,2048]{2,1,0:T(8,128)(2,1)S(1)}, bf16[1,2048,2048]{2,1,0:T(8,128)(2,1)}, u32[]{:S(2)}) copy-start(bf16[1,2048,2048]{2,1,0:T(8,128)(2,1)} %all-gather.14.cloned.1.call-done) | copy-start | bytes 25165828
  248.8 1.2 copy-start.1
  252.7 0.8 copy-start.2
  322.5 128.1 %all-gather.10.cloned.1.call-start = ((), (), s32[]{:S(2)}) async-start(), calls=%async_computation.3 | async-start | bytes 8912896 | tf_op jit(solution)/shard_map/all_gather | solution.py:321
Sparse Core Ops, SparseCore 0:
  8.9 109.3 all-gather.11
  120.2 71.9 all-gather.15
  193.7 20.7 all-gather.13
  322.6 15.4 all-gather.17
  340.7 109.9 all-gather.9

commit v2 on v1

--- a/solution.py
+++ b/solution.py
@@ -1,6 +1,8 @@
 import jax
 import jax.numpy as jnp
 from jax import lax
+from jax.experimental import pallas as pl
+from jax.experimental.pallas import tpu as pltpu
 from jax.sharding import PartitionSpec as P
 
 DK = 64
@@ -229,6 +231,93 @@
     return ((before, ceiling), cumulative, inputs)
 
 
+def spread_kernel(first, second, n, m, x_ref, out_ref, local_sem, send, recv, send_on, recv_on):
+    me = lax.axis_index(first)
+    mine = lax.axis_index(second)
+    barrier = pltpu.get_barrier_semaphore()
+    mesh_ids = pl.DeviceIdType.MESH
+    for k in range(1, n):
+        pl.semaphore_signal(
+            barrier, inc=1, device_id={first: lax.rem(me + k, n)}, device_id_type=mesh_ids
+        )
+    for k in range(1, m):
+        pl.semaphore_signal(
+            barrier, inc=1, device_id={second: lax.rem(mine + k, m)}, device_id_type=mesh_ids
+        )
+    pl.semaphore_wait(barrier, n + m - 2)
+    copies = []
+    for k in range(1, n):
+        peer = lax.rem(me + k, n)
+        copy = pltpu.make_async_remote_copy(
+            src_ref=x_ref.at[peer],
+            dst_ref=out_ref.at[me, mine],
+            send_sem=send.at[k - 1],
+            recv_sem=recv.at[k - 1],
+            device_id={first: peer},
+            device_id_type=mesh_ids,
+        )
+        copy.start()
+        copies.append(copy)
+    kept = pltpu.make_async_copy(x_ref.at[me], out_ref.at[me, mine], local_sem)
+    kept.start()
+    onward = []
+    for k in range(n):
+        source = lax.rem(me - k + n, n)
+        if k > 0:
+            copies[k - 1].wait_recv()
+        block = x_ref.at[me] if k == 0 else out_ref.at[source, mine]
+        for j in range(1, m):
+            copy = pltpu.make_async_remote_copy(
+                src_ref=block,
+                dst_ref=out_ref.at[source, mine],
+                send_sem=send_on.at[k, j - 1],
+                recv_sem=recv_on.at[k, j - 1],
+                device_id={second: lax.rem(mine + j, m)},
+                device_id_type=mesh_ids,
+            )
+            copy.start()
+            onward.append(copy)
+    kept.wait()
+    for copy in copies:
+        copy.wait_send()
+    for k in range(n):
+        for j in range(1, m):
+            copy = onward[k * (m - 1) + j - 1]
+            copy.wait_send()
+            copy.wait_recv()
+
+
+def spread(x, first, second, number):
+    n, m = lax.axis_size(first), lax.axis_size(second)
+    shape = (n, m) + x.shape[1:]
+    size = x.size * x.dtype.itemsize * m
+    return pl.pallas_call(
+        lambda *refs: spread_kernel(first, second, n, m, *refs),
+        out_shape=jax.ShapeDtypeStruct(shape, x.dtype),
+        in_specs=[pl.BlockSpec(memory_space=pltpu.VMEM)],
+        out_specs=pl.BlockSpec(memory_space=pltpu.VMEM),
+        scratch_shapes=[
+            pltpu.SemaphoreType.DMA,
+            pltpu.SemaphoreType.DMA((n - 1,)),
+            pltpu.SemaphoreType.DMA((n - 1,)),
+            pltpu.SemaphoreType.DMA((n, m - 1)),
+            pltpu.SemaphoreType.DMA((n, m - 1)),
+        ],
+        compiler_params=pltpu.CompilerParams(collective_id=number, has_side_effects=True),
+        cost_estimate=pl.CostEstimate(flops=0, bytes_accessed=30 * size, transcendentals=0),
+    )(x)
+
+
+def both_halves(own, axis):
+    if lax.axis_size("tp") != 2:
+        return lax.all_gather(own, "tp", axis=axis, tiled=True)
+    other = lax.ppermute(own, "tp", [(0, 1), (1, 0)])
+    first = lax.axis_index("tp") == 0
+    return jnp.concatenate(
+        [jnp.where(first, own, other), jnp.where(first, other, own)], axis=axis
+    )
+
+
 def resharded(
     tokens,
     norm_gain,
@@ -259,15 +348,24 @@
         exit_weight,
         entry_weight,
         signal_weight,
-        gate_weight.reshape(depth, 2, parts, heads).transpose(0, 2, 1, 3),
+        gate_weight.reshape(depth, 2, parts, heads).swapaxes(1, 2).reshape(depth, -1),
     ]
-    stacked = jnp.concatenate([w.reshape(depth, parts, -1) for w in stack], axis=2)
     widths = [w.size // depth // parts for w in stack]
-    sent = lax.all_to_all(stacked.transpose(1, 0, 2), "sp", 0, 0)
-    rows = lax.all_gather(sent, "fs", axis=1)
+    spare = jnp.zeros((depth, -sum(widths) % 128), jnp.bfloat16)
+    stacked = jnp.stack(
+        [
+            jnp.concatenate(
+                [w[:, p * width : (p + 1) * width] for w, width in zip(stack, widths)] + [spare],
+                axis=1,
+            )
+            for p in range(parts)
+        ]
+    )
+    rows = spread(stacked, "sp", "fs", 0)
     rows = rows.reshape(-1, rows.shape[-1])
     line = lax.all_gather(tokens[0], "sp", axis=0, tiled=True)
-    whole = lax.all_gather(line, "tp", axis=1, tiled=True)
+    rows, line, merge_weight = lax.optimization_barrier((rows, line, merge_weight))
+    whole = both_halves(line, 1)
     count = whole.shape[0]
     flat = whole.astype(jnp.float32)
     normed = (
@@ -313,13 +411,16 @@
         own(head_norm_gain, 0, heads * DV),
     )
     both = jnp.concatenate([memory_out, conv_out], axis=1)
-    back = lax.all_to_all(both.reshape(parts, count // parts, -1), "sp", 0, 0)
-    halves = lax.all_gather(back, "tp")
+    halves = spread(both.reshape(parts, count // parts, -1), "sp", "tp", 1)
     memory_width = heads * DV
-    memory_all = halves[..., :memory_width].transpose(2, 0, 1, 3).reshape(count // parts, -1)
-    conv_all = halves[..., memory_width:].transpose(2, 0, 1, 3).reshape(count // parts, -1)
+    pieces = [(t, p) for t in range(halves.shape[1]) for p in range(parts)]
+    merged_in = jnp.concatenate(
+        [halves[p, t, :, :memory_width] for t, p in pieces]
+        + [halves[p, t, :, memory_width:] for t, p in pieces],
+        axis=1,
+    )
     merge = lax.all_gather(merge_weight, ("sp", "fs"), axis=0, tiled=True)
-    mixed = add_product(jnp.concatenate([memory_all, conv_all], axis=1), merge)
+    mixed = add_product(merged_in, merge)
     return mixed.astype(jnp.bfloat16)[None]
 
 
@@ -345,8 +446,9 @@
 
     def step(*args):
         heads, channels = args[6].shape[2], args[10].shape[1]
+        many = min(sp, mesh.shape["fs"], tp) > 1
         even = heads % (sp * tp) == 0 and channels % (sp * tp * 128) == 0
-        body = resharded if even else local
+        body = resharded if many and even else local
         return jax.shard_map(
             body, mesh=mesh, in_specs=placed, out_specs=P("fs", "sp", "tp"), check_vma=False
         )(*args)

time: 472 us -> 347 us (0.74)
  waiting for transfers between devices: 210 us -> 5.93 us
  Pallas kernels: 0 us -> 195 us
  blocking collectives: 129 us -> 0 us
  starting transfers between devices: 6.5 us -> 24 us
  local copies, waits for them, and re-layouts: 52.9 us -> 45.1 us
  matrix products: 37.7 us -> 42.5 us
    pallas_call x0 -> x2, Pallas kernels: none -> 195 us  [spread(): pl.pallas_call(lambda *refs: spread_kernel(first, second, n, m, *refs), o...]
    all_to_all x2 -> x0, blocking collectives: 129 us -> none  [the longest x1 79 us: resharded(): sent = lax.all_to_all(stacked.transpose(1, 0, 2), 'sp', 0, 0)]
    all_gather x1, waiting for transfers between devices: 102 us -> 0.01 us  [resharded(): merge = lax.all_gather(merge_weight, ('sp', 'fs'), axis=0, tiled=True)]
    all_gather x3 -> x0, waiting for transfers between devices: 79.3 us -> none  [the longest x1 64.3 us: resharded(): rows = lax.all_gather(sent, 'fs', axis=1)]
    all_gather x2 -> x0, local copies, waits for them, and re-layouts: 24.1 us -> none  [the longest x1 17.7 us: resharded(): rows = lax.all_gather(sent, 'fs', axis=1)]
    all_gather x1, waiting for transfers between devices: 27.7 us -> 5.2 us  [resharded(): line = lax.all_gather(tokens[0], 'sp', axis=0, tiled=True)]
    all_to_all x1, starting transfers between devices: 6.34 us -> 23.6 us  [resharded(): lax.all_to_all(forget_shift[0].reshape(parts, heads, -1), 'sp', 0, 0)]
    unnamed x46 -> x41, local copies, waits for them, and re-layouts: 17.2 us -> 30.7 us
  transfers between devices with their start and end apart: 6 -> 4, of which waited for: 4 -> 1; matrix products, arithmetic and copies ran while one was open for 14% -> 28% of each run, Pallas kernels for 0% -> 56%
where the time goes in v2:
time: 347 us; the launch traced here: 346 us
  Pallas kernels  195 us (56%)
  local copies, waits for them, and re-layouts  45.1 us (13%)
  matrix products  42.5 us (12%)
  starting transfers between devices  24 us (7%)
  other arithmetic  19.2 us (6%)
  between operations  13.8 us (4%)
  waiting for transfers between devices  5.93 us (2%)
    pallas_call x2, Pallas kernels, spread(): pl.pallas_call(lambda *refs: spread_kernel(first, second, n, m, *refs), o...  195 us
    dot_general x2, matrix products, add_product(): return jnp.dot(left, piece, preferred_element_type=jnp.float32)  33.2 us
    unnamed x41, local copies, waits for them, and re-layouts  30.7 us
    all_to_all x1, starting transfers between devices, resharded(): lax.all_to_all(forget_shift[0].reshape(parts, heads, -1), 'sp', 0, 0)  23.6 us
  transfers between devices with their start and end apart: 4, of which 1 were waited for; matrix products, arithmetic and copies ran while one was open for 28% of the time, Pallas kernels for 56%

profile of v2, /device:TPU:9, one launch (start us, length us, event | category | flops | bytes accessed | tf_op | source)
XLA Modules:
  0.0 345.6 jit_solution(6777703396418532237)
XLA Ops:
  6.5 0.7 all-gather.6.cloned.1.call-update
  7.3 0.7 copy.130
  8.5 1.0 fusion.71
  9.5 0.9 fusion.72
  10.4 1.1 fusion.67
  11.5 1.1 fusion.69
  13.1 1.5 pad_maximum_fusion.3.refs_0_
  14.6 103.1 %shard_map.145 = bf16[4,4,128,1664]{3,2,1,0:T(8,128)(2,1)} custom-call(bf16[4,128,1664]{2,1,0:T(8,128)(2,1)} %pad_maximum_fusion.3.refs_0_), custom_call_target="tpu_custom_call" | custom-call | bytes 204472320 | tf_op jit(solution)/shard_map/pallas_call | solution.py:294
  117.7 5.2 %all-gather.6.cloned.1.call-done = bf16[1,2048,1024]{2,1,0:T(8,128)(2,1)} async-done(((bf16[1,512,1024]{2,1,0:T(8,128)(2,1)}), bf16[1,2048,1024]{2,1,0:T(8,128)(2,1)}) %all-gather.6.cloned.1.call-update) | async-done | bytes 4194320 | tf_op jit(solution)/shard_map/all_gather | solution.py:366
  124.0 23.6 %all-to-all-start = ((f32[4,2,512]{2,1,0:T(2,128)}), f32[4,2,512]{2,1,0:T(2,128)S(1)}, u32[]{:S(2)}, u32[]{:S(2)}) async-start(f32[4,2,512]{2,1,0:T(2,128)} %reshape_squeeze.3), calls=%async_computation | async-start | bytes 32768 | tf_op jit(solution)/shard_map/all_to_all | solution.py:388
  147.7 0.8 dynamic_slice.10
  148.4 0.9 constant_dynamic-slice_fusion
  149.4 3.9 %broadcast_select_fusion.1 = (bf16[2048,1024]{1,0:T(8,128)(2,1)S(1)}, bf16[2048,1024]{1,0:T(8,128)(2,1)S(1)}) fusion(bf16[2048,1024]{1,0:T(8,128)(2,1)} %bitcast.138, bf16[2048,1024]{1,0:T(8,128)(2,1)} %collective-permute-done, pred[]{:T(512)S(6)} %eq.3), kind=kLoop, calls=%fused_computation.10 | loop fusion | flops 4194304 | bytes 16777216 | tf_op jit(solution)/shard_map/jit(_where)/select_n | solution.py:317
  153.3 1.9 fusion
  155.3 1.3 copy-done.1
  156.6 23.1 %fusion.75 = (bf16[2048,1664]{0,1:T(8,128)(2,1)}, f32[2048,1664]{0,1:T(8,128)}) fusion(bf16[2048,1664]{1,0:T(8,128)(2,1)} %bitcast.136, f32[2048]{0:T(1024)S(1)} %copy-done.5, f32[2048]{0:T(1024)S(1)} %add_rsqrt_fusion, bf16[2048,1024]{1,0:T(8,128)(2,1)} %copy-done.1, bf16[2048,1024]{1,0:T(8,128)(2,1)} %copy-done), kind=kOutput, calls=%fused_computation.129 | convolution fusion | flops 13991411712 | bytes 35667968 | tf_op jit(solution)/shard_map/dot_general | solution.py:55
  179.7 1.0 fusion.46
  181.9 1.3 fusion.15
  183.5 1.3 slice_bitcast_fusion
  185.0 1.1 copy.152
  186.1 1.3 slice_bitcast_fusion.2
  187.7 1.0 fusion.21
  188.6 1.6 convolution_bitcast_fusion
  190.3 1.9 fusion.18
  192.2 4.6 %multiply_reduce_fusion = (f32[16,2,128]{2,1,0:T(2,128)S(1)}, f32[16,2,128,128]{2,3,1,0:T(8,128)}) fusion(f32[16,2,128,128]{2,3,1,0:T(8,128)S(1)} %fusion.18, f32[16,2,128]{2,1,0:T(2,128)S(1)} %copy.157, bf16[16,128,2,128]{3,1,2,0:T(8,128)(2,1)S(1)} %copy.152, f32[16,2,128]{2,1,0:T(2,128)S(1)} %copy.145, f32[16,2,128]{2,1,0:T(2,128)S(1)} %copy.139, ...), kind=kOutput, calls=%fused_computation.26 | convolution fusion | flops 207089664 | bytes 6389760 | tf_op jit(solution)/shard_map/chjs,cshv->chjv/dot_general | solution.py:124
  196.8 2.1 fusion.14
  198.9 1.2 copy.158
  200.2 3.3 fusion.8
  203.8 2.7 fusion.11
  207.0 2.5 copy.159
  209.5 91.9 %shard_map.146 = bf16[4,2,512,512]{3,2,1,0:T(8,128)(2,1)} custom-call(bf16[4,512,512]{2,1,0:T(8,128)(2,1)} %bitcast.134), custom_call_target="tpu_custom_call" | custom-call | bytes 125829120 | tf_op jit(solution)/shard_map/pallas_call | solution.py:294
  301.4 1.7 bitcast_dynamic-update-slice_fusion.15
  303.1 1.7 bitcast_dynamic-update-slice_fusion.14
  304.8 1.7 bitcast_dynamic-update-slice_fusion.13
  306.5 1.7 bitcast_dynamic-update-slice_fusion.12
  308.2 1.7 bitcast_dynamic-update-slice_fusion.11
  309.9 1.7 bitcast_dynamic-update-slice_fusion.10
  311.6 1.7 bitcast_dynamic-update-slice_fusion.9
  313.3 1.7 bitcast_dynamic-update-slice_fusion.8
  315.0 1.7 bitcast_dynamic-update-slice_fusion.7
  316.7 1.7 bitcast_dynamic-update-slice_fusion.6
  318.4 1.7 bitcast_dynamic-update-slice_fusion.5
  320.1 1.7 bitcast_dynamic-update-slice_fusion.4
  321.8 1.7 bitcast_dynamic-update-slice_fusion.3
  323.5 1.7 bitcast_dynamic-update-slice_fusion.2
  325.2 1.7 bitcast_dynamic-update-slice_fusion.1
  326.9 1.7 bitcast_dynamic-update-slice_fusion
  328.7 10.1 %fusion.17 = bf16[1,512,1024]{2,1,0:T(8,128)(2,1)} fusion(bf16[512,4096]{1,0:T(8,128)(2,1)} %bitcast_dynamic-update-slice_fusion, bf16[4096,1024]{1,0:T(8,128)(2,1)} %all-gather.4.cloned.1.call-done), kind=kOutput, calls=%fused_computation.33 | convolution fusion | flops 4295491584 | bytes 13631488 | tf_op jit(solution)/shard_map/dot_general | solution.py:55
  (60 shorter events, 4.9 us)
Async XLA Ops:
  6.5 116.4 %all-gather.6.cloned.1.call-start = ((), (), s32[]{:S(2)}) async-start(), calls=%async_computation.2 | async-start | bytes 5242880 | tf_op jit(solution)/shard_map/all_gather | solution.py:366
  7.3 321.4 %all-gather.4.cloned.1.call-start = ((), (), s32[]{:S(2)}) async-start(), calls=%async_computation.1 | async-start | bytes 8912896 | tf_op jit(solution)/shard_map/all_gather | solution.py:422
  14.6 108.8 %copy-start.4 = (f32[1,8,512]{2,1,0:T(8,128)S(1)}, f32[1,8,512]{2,1,0:T(8,128)}, u32[]{:S(2)}) copy-start(f32[1,8,512]{2,1,0:T(8,128)} %param.23) | copy-start | bytes 49156
  14.6 133.0 %copy-start.6 = (f32[8]{0:T(128)S(1)}, f32[8]{0:T(128)}, u32[]{:S(2)}) copy-start(f32[8]{0:T(128)} %param.22) | copy-start | bytes 100
  122.9 26.4 %collective-permute-start = (bf16[2048,1024]{1,0:T(8,128)(2,1)}, bf16[2048,1024]{1,0:T(8,128)(2,1)}, u32[]{:S(2)}, u32[]{:S(2)}) collective-permute-start(bf16[2048,1024]{1,0:T(8,128)(2,1)} %bitcast.137), channel_id=1, source_target_pairs={{0,1},{1,0},{2,3},{3,2},{4,5},{5,4},{6,7},{7,6},{8,9},{9,8},{10,11... | collective-permute-start | bytes 12582920 | tf_op jit(solution)/shard_map/ppermute | solution.py:314
  124.0 55.7 %all-to-all-start = ((f32[4,2,512]{2,1,0:T(2,128)}), f32[4,2,512]{2,1,0:T(2,128)S(1)}, u32[]{:S(2)}, u32[]{:S(2)}) async-start(f32[4,2,512]{2,1,0:T(2,128)} %reshape_squeeze.3), calls=%async_computation | async-start | bytes 32768 | tf_op jit(solution)/shard_map/all_to_all | solution.py:388
  153.3 2.0 copy-start
  153.3 3.3 copy-start.1
  153.3 3.3 copy-start.5
  187.5 2.8 copy-start.2
  187.6 2.6 copy-start.3
Sparse Core Ops, SparseCore 0:
  8.9 113.9 all-gather.5
  125.7 165.7 all-gather.3
